TPU v7x, 32 devices: a whole 2x2x4 slice. The times are simulated.
32 devices in a mesh: sp: 4 (over z), fs: 4 (over y, x), tp: 2 (over core).
Axes of the slice: x: 2, y: 2, z: 4, core: 2. Of those that a mesh axis runs over, the one named last changes fastest.
Arguments:
- tokens: bfloat16 [2048, 2048], P(('fs', 'sp')), may hold values from -6 to 6
- in_gain: float32 [2048], replicated, may hold values from 0.1 to 1.9
- query_weight: bfloat16 [2048, 512], P(None, ('tp', 'fs')), may hold values from -0.17291713 to 0.17291713
- key_weight: bfloat16 [2048, 512], P(None, ('tp', 'fs')), may hold values from -0.17291713 to 0.17291713
- value_weight: bfloat16 [2048, 512], P(None, ('tp', 'fs')), may hold values from -0.125 to 0.125
- rec_query_weight: bfloat16 [2048, 512], P(None, ('tp', 'fs')), may hold values from -0.125 to 0.125
- rec_forget_weight: bfloat16 [2048, 512], P(None, ('tp', 'fs')), may hold values from -0.125 to 0.125
- rec_input_weight: bfloat16 [2048, 512], P(None, ('tp', 'fs')), may hold values from -0.125 to 0.125
- mix_lambda: float32 [4], P('tp'), may hold values from 0.3 to 0.8
- lower_bound: float32 [4, 128], P('tp'), may hold values from 0.9 to 0.9995117
- forget_scale: float32 [2048], P(('fs', 'sp')), may hold values from 0.35 to 1536
- att_gain: float32 [128], replicated, may hold values from 0.1 to 1.9
- recurrence_gain: float32 [128], replicated, may hold values from 0.1 to 1.9
- att_out_weight: bfloat16 [512, 2048], P('tp'), may hold values from -0.1875 to 0.1875
- rec_out_weight: bfloat16 [512, 2048], P('tp'), may hold values from -0.1875 to 0.1875
Outputs:
- mixed_out: bfloat16 [2048, 2048], P(('fs', 'sp'))
- log_weight_sum: float32 [4, 2048], P('tp', ('fs', 'sp'))
All inputs are finite; a program needn't handle non-finite values.
Results may differ from a plain program's by a relative error of at most 0.012.
Values may be sent and summed in bfloat16 or wider, within the bound.
A program may use at most 128 MiB of HBM per device.

v0:
```python
import jax
import jax.numpy as jnp
from jax import lax
from jax.sharding import PartitionSpec as P

DK = 64
DV = 128
BLK = 64


EPS = 1e-06
NEG = -1e30


def from_behind(value, axis, steps):
    count = lax.axis_size(axis)
    initial, last = (max(0, -steps), min(count, count - steps))
    return lax.ppermute(value, axis, [(source, source + steps) for source in range(initial, last)])


def entering(value, axis, join, neutral):
    count, mine = (lax.axis_size(axis), lax.axis_index(axis))
    pieces = jax.tree.map(lambda part: lax.all_gather(part, axis), value)
    running = jax.tree.map(
        lambda part, zero: jnp.full_like(part, 0) + jnp.asarray(zero, part.dtype), value, neutral
    )

    def step(position, running):
        longer = join(running, jax.tree.map(lambda part: part[position], pieces))
        return jax.tree.map(lambda new, old: jnp.where(position < mine, new, old), longer, running)

    return lax.fori_loop(0, count - 1, step, running)


def norm_rows(values, gain):
    return values * lax.rsqrt(jnp.mean(values * values, axis=-1, keepdims=True) + EPS) * gain


def block_recurrence(queries, key_in, value_in, log_forget):
    head_count, row_count, key_width = queries.shape
    block_count = row_count // BLK

    def to_blocks(array_in):
        return array_in.reshape(head_count, block_count, BLK, array_in.shape[-1]).transpose(
            1, 0, 2, 3
        )

    causal = jnp.tril(jnp.ones((BLK, BLK), bool))

    def advance(passed_state, inputs):
        query_block, key_block, value_block, l_blk = inputs
        accumulator_sum = jnp.cumsum(l_blk, axis=1)
        cross_block_output = jnp.einsum(
            "sre,sei->sri",
            query_block * jnp.exp(accumulator_sum),
            passed_state,
            precision=lax.Precision.HIGHEST,
        )
        spread = accumulator_sum[:, :, None, :] - accumulator_sum[:, None, :, :]
        decay = jnp.exp(jnp.where(causal[None, :, :, None], spread, -jnp.inf))
        scores = jnp.einsum(
            "htk,htsk,hsk->hts", query_block, decay, key_block, precision=lax.Precision.HIGHEST
        )
        result = cross_block_output + jnp.einsum(
            "hts,hsv->htv", scores, value_block, precision=lax.Precision.HIGHEST
        )
        final_log_sum = accumulator_sum[:, -1:, :]
        updated_state = jnp.exp(final_log_sum[:, 0, :])[:, :, None] * passed_state + jnp.einsum(
            "plf,plt->pft",
            key_block * jnp.exp(final_log_sum - accumulator_sum),
            value_block,
            precision=lax.Precision.HIGHEST,
        )
        return (updated_state, result)

    begin_state = jnp.zeros((head_count, key_width, value_in.shape[-1]), jnp.float32)
    end_state, results = lax.scan(
        advance,
        begin_state,
        (to_blocks(queries), to_blocks(key_in), to_blocks(value_in), to_blocks(log_forget)),
    )
    return (
        end_state,
        results.transpose(1, 0, 2, 3).reshape(head_count, row_count, value_in.shape[-1]),
    )


def attend(online, queries, pair_keys, pair_values, allowed):
    running_max, weight_sum, numer_sum = online
    local_heads = numer_sum.shape[0]
    key_rows = pair_keys.shape[0]
    key_heads = pair_keys.reshape(key_rows, local_heads, 2, DK).transpose(1, 2, 0, 3)
    head_values = pair_values.reshape(key_rows, local_heads, DV).transpose(1, 0, 2)
    scores = jnp.einsum(
        "hmqd,hmkd->hmqk", queries, key_heads, preferred_element_type=jnp.float32
    ) * DK ** (-0.5)
    scores = jnp.where(allowed, scores, NEG)
    highest = jnp.maximum(running_max, jnp.max(scores, axis=-1))
    weights = jnp.exp(scores - highest[..., None])
    shrink = jnp.exp(running_max - highest)
    weight_sum = weight_sum * shrink + jnp.sum(weights, axis=-1)
    numer_sum = numer_sum * shrink[..., None] + jnp.einsum(
        "itap,ipn->itan",
        weights.astype(jnp.bfloat16),
        head_values,
        preferred_element_type=jnp.float32,
    )
    return (highest, weight_sum, numer_sum)


def attend_pieces(online, queries, pieces, first_offset, position):

    def visit(piece_index, inner):
        piece = lax.dynamic_index_in_dim(pieces, piece_index, 0, keepdims=False)
        return lax.cond(
            position >= first_offset + piece_index,
            lambda state: attend(state, queries, piece[0], piece[1], True),
            lambda state: state,
            inner,
        )

    return lax.fori_loop(0, pieces.shape[0], visit, online)


def on_device(
    tokens,
    in_gain,
    query_weight,
    key_weight,
    value_weight,
    rec_query_weight,
    rec_forget_weight,
    rec_input_weight,
    mix_lambda,
    lower_bound,
    forget_scale,
    att_gain,
    recurrence_gain,
    att_out_weight,
    rec_out_weight,
):
    normed = norm_rows(tokens.astype(jnp.float32), in_gain).astype(jnp.bfloat16)
    row_count = normed.shape[0]
    stacked = jnp.stack(
        [
            query_weight,
            key_weight,
            value_weight,
            rec_query_weight,
            rec_forget_weight,
            rec_input_weight,
        ],
        axis=1,
    )
    projected = jnp.einsum(
        "rd,dnc->rnc",
        normed,
        lax.all_gather(stacked, "fs", axis=2, tiled=True),
        preferred_element_type=jnp.float32,
    ).astype(jnp.bfloat16)
    local_heads = projected.shape[2] // DV
    position = lax.axis_index("sp")
    queries = projected[:, 0].reshape(row_count, local_heads, 2, DK).transpose(1, 2, 0, 3)
    online = (
        jnp.full((local_heads, 2, row_count), NEG, jnp.float32),
        jnp.zeros((local_heads, 2, row_count), jnp.float32),
        jnp.zeros((local_heads, 2, row_count, DV), jnp.float32),
    )
    moving = jnp.stack([projected[:, 1], projected[:, 2]])
    causal = jnp.arange(row_count)[:, None] >= jnp.arange(row_count)[None, :]
    online = attend(online, queries, moving[0], moving[1], causal)
    buffer = moving[None]
    levels = (lax.axis_size("sp") - 1).bit_length()
    offset_now = 1
    for level_index in range(levels):
        received = from_behind(buffer, "sp", offset_now)
        online = attend_pieces(online, queries, received, offset_now, position)
        if level_index + 1 < levels:
            buffer = jnp.concatenate([buffer, received], axis=0)
        offset_now = offset_now * 2
    running_max, weight_sum, numer_sum = online
    mixed_heads = (
        numer_sum[:, 0] / weight_sum[:, 0, :, None]
        - mix_lambda[:, None, None] * numer_sum[:, 1] / weight_sum[:, 1, :, None]
    )
    att_heads = (norm_rows(mixed_heads, att_gain) * 0.8).astype(jnp.bfloat16)
    att_rows = att_heads.transpose(1, 0, 2).reshape(row_count, local_heads * DV)
    log_weight_sum = running_max[:, 0] + jnp.log(weight_sum[:, 0])

    def heads_first(array_in):
        return array_in.reshape(row_count, local_heads, DV).transpose(1, 0, 2).astype(jnp.float32)

    recurrent_queries = heads_first(projected[:, 3])
    lower_edge = lower_bound[:, None, :]
    forget = lower_edge + (1.0 - lower_edge) * jax.nn.sigmoid(heads_first(projected[:, 4]))
    log_forget = forget_scale[None, :, None] * jnp.log(forget)
    key_in = 1.0 - jnp.exp(log_forget)
    end_state, local_result = block_recurrence(
        recurrent_queries, key_in, heads_first(projected[:, 5]), log_forget
    )
    running_state = jnp.cumsum(log_forget, axis=1)
    carry_rate = jnp.exp(running_state[:, -1, :])

    def combine(earlier, later):
        return (later[0] * earlier[0], later[0][..., None] * earlier[1] + later[1])

    identity = (jnp.ones_like(carry_rate), jnp.zeros_like(end_state))
    _, incoming_state = entering((carry_rate, end_state), "sp", combine, identity)
    combined = local_result + jnp.einsum(
        "zed,zdp->zep",
        recurrent_queries * jnp.exp(running_state),
        incoming_state,
        precision=lax.Precision.HIGHEST,
    )
    rec_heads = norm_rows(combined, recurrence_gain).astype(jnp.bfloat16)
    rec_rows = rec_heads.transpose(1, 0, 2).reshape(row_count, local_heads * DV)
    partial_value = jnp.dot(att_rows, att_out_weight, preferred_element_type=jnp.float32) + jnp.dot(
        rec_rows, rec_out_weight, preferred_element_type=jnp.float32
    )
    mixed_out = lax.psum(partial_value.astype(jnp.bfloat16), "tp")
    return (mixed_out, log_weight_sum)


def solution(mesh):
    return jax.shard_map(
        on_device,
        mesh=mesh,
        in_specs=(
            P(("fs", "sp"), None),
            P(),
            P(None, ("tp", "fs")),
            P(None, ("tp", "fs")),
            P(None, ("tp", "fs")),
            P(None, ("tp", "fs")),
            P(None, ("tp", "fs")),
            P(None, ("tp", "fs")),
            P("tp"),
            P("tp", None),
            P(("fs", "sp")),
            P(),
            P(),
            P("tp", None),
            P("tp", None),
        ),
        out_specs=(P(("fs", "sp"), None), P("tp", ("fs", "sp"))),
        check_vma=False,
    )
```

profile of v0, /device:TPU:25, one launch (start us, length us, event | category | flops | bytes accessed | tf_op | source)
XLA Modules:
  0.0 176.0 jit_solution(9279672745273595247)
XLA Ops:
  7.3 1.1 bitcast_dynamic-update-slice_fusion.5
  8.3 1.0 bitcast_dynamic-update-slice_fusion.4
  9.3 1.0 bitcast_dynamic-update-slice_fusion.3
  10.5 1.1 copy-done.1
  11.7 0.2 fusion.46
  11.9 70.7 %all-gather.4.cloned.1.call-done = bf16[2048,6,256]{0,2,1:T(8,128)(2,1)} async-done(((bf16[2048,6,64]{0,2,1:T(8,128)(2,1)}), bf16[2048,6,256]{0,2,1:T(8,128)(2,1)}) %all-gather.4.cloned.1.call-update) | async-done | bytes 6291472 | tf_op jit(solution)/shard_map/all_gather | solution.py:158
  82.6 5.0 %convolution_convert_fusion = bf16[128,6,256]{2,0,1:T(8,128)(2,1)S(1)} fusion(bf16[2048,6,256]{0,2,1:T(8,128)(2,1)} %all-gather.4.cloned.1.call-done, bf16[128,2048]{1,0:T(8,128)(2,1)S(1)} %copy-done.2, f32[2048]{0:T(1024)S(1)} %copy-done.7, f32[128]{0:T(128)S(1)} %add_rsqrt_fusion.2), kind=kOutput, calls=%fused_computation.66 | convolution fusion | flops 806551552 | bytes 7217664 | tf_op jit(solution)/shard_map/rd,dnc->rnc/dot_general | solution.py:155
  87.7 0.1 copy.61
  87.8 0.1 copy.62
  88.0 0.3 fusion.75
  88.2 0.1 fusion.54
  88.4 1.3 collective-permute-start
  89.7 0.1 reshape.122
  89.8 0.1 reshape.123
  89.9 0.1 reshape.120
  90.0 0.1 exponential_subtract_fusion
  90.1 16.1 %while.52 = (s32[]{:T(128)}, f32[2,128,128]{2,1,0:T(8,128)S(1)}, f32[2,2,64,128]{3,2,0,1:T(8,128)S(1)}, f32[2,2,64,128]{3,2,0,1:T(8,128)S(1)}, f32[2,2,64,128]{3...) while((s32[]{:T(128)}, f32[2,128,128]{2,1,0:T(8,128)S(1)}, ...), condition=%wide.region_16.17_spmd.clone, body=%wide.region_14.16_spmd.clone.sunk | while | flops 79876096 | bytes 1818748 | solution.py:77
  90.1 0.1 reduce_window_sum.25
  90.2 7.0 %fusion.110 = f32[2,64,1,64]{3,2,1,0:T(1,128)S(1)} fusion(f32[2,64,128,1]{2,3,1,0:T(1,128)S(1)} %bitcast.210, f32[2,64,128]{2,1,0:T(8,128)S(1)} %get-tuple-element.685, f32[2,64,128]{2,1,0:T(8,128)S(1)} %reduce_window_sum.25, pred[64,64]{1,0:T(8,128)(4,1)S(1)} %iota_compare_fusion.3), kind=kOutput, calls=%fused_computation.22.clone.1 | convolution fusion | flops 15728640 | bytes 233472 | tf_op jit(solution)/shard_map/while/body/eval_jaxpr/htk,htsk,hsk->hts/dot_general | solution.py:61
  97.2 0.3 fusion.109
  97.5 0.2 fusion.111
  97.7 0.4 convolution_add_fusion.8
  98.2 0.1 reduce_window_sum.25
  98.3 7.0 %fusion.110 = f32[2,64,1,64]{3,2,1,0:T(1,128)S(1)} fusion(f32[2,64,128,1]{2,3,1,0:T(1,128)S(1)} %bitcast.210, f32[2,64,128]{2,1,0:T(8,128)S(1)} %get-tuple-element.685, f32[2,64,128]{2,1,0:T(8,128)S(1)} %reduce_window_sum.25, pred[64,64]{1,0:T(8,128)(4,1)S(1)} %iota_compare_fusion.3), kind=kOutput, calls=%fused_computation.22.clone.1 | convolution fusion | flops 15728640 | bytes 233472 | tf_op jit(solution)/shard_map/while/body/eval_jaxpr/htk,htsk,hsk->hts/dot_general | solution.py:61
  105.3 0.3 fusion.109
  105.5 0.2 fusion.111
  105.8 0.4 convolution_add_fusion.8
  106.2 13.3 %all-gather.1 = f32[8,128,128]{2,1,0:T(8,128)S(1)} all-gather(f32[2,128,128]{2,1,0:T(8,128)S(1)} %get-tuple-element.398), channel_id=3, replica_groups=mesh['sp'=4,'fs'=4,'tp'=2] {'sp'}, dimensions={0}, use_global_device_ids=true | all-gather | bytes 655360 | tf_op jit(solution)/shard_map/all_gather | solution.py:23
  119.5 0.2 reduce_window_sum.22
  119.7 5.6 %all-gather = f32[8,1,128]{2,1,0:T(1,128)S(1)} all-gather(f32[2,1,128]{2,1,0:T(1,128)S(1)} %slice_exponential_fusion), channel_id=2, replica_groups=mesh['sp'=4,'fs'=4,'tp'=2] {'sp'}, dimensions={0}, use_global_device_ids=true | all-gather | bytes 5120 | tf_op jit(solution)/shard_map/all_gather | solution.py:23
  125.3 0.5 while.53
  125.3 0.1 fusion.112
  125.5 0.1 fusion.112
  125.7 0.1 fusion.112
  125.8 0.1 copy.79
  125.9 0.4 multiply_reduce_fusion
  126.3 0.2 convolution_add_fusion.5
  126.6 1.3 collective-permute-start.1
  127.9 0.1 multiply_convert_fusion
  128.0 0.9 conditional.2
  128.1 0.1 copy.65
  128.2 0.3 fusion.73
  128.5 0.1 copy.57
  128.7 0.3 convolution_add_fusion
  129.0 8.5 %collective-permute-done.1 = bf16[2,2,128,256]{3,2,1,0:T(8,128)(2,1)S(1)} collective-permute-done((bf16[2,2,128,256]{3,2,1,0:T(8,128)(2,1)S(1)}, bf16[2,2,128,256]{3,2,1,0:T(8,128)(2,1)S(1)}, u32[]{:S(2)}, u32[]{:S(2)}) %collective-permute-start.1) | collective-permute-done | bytes 262176 | tf_op jit(solution)/shard_map/ppermute | solution.py:18
  137.4 0.2 copy.66
  137.6 1.7 while.51
  137.7 0.8 conditional.4
  137.7 0.3 fusion.74
  138.1 0.1 copy.59
  138.2 0.3 convolution_add_fusion.1
  138.5 0.8 conditional.4
  138.6 0.3 fusion.74
  138.9 0.1 copy.59
  139.0 0.3 convolution_add_fusion.1
  139.4 0.1 copy.67
  139.6 0.1 multiply_reduce_fusion.1
  139.7 0.1 multiply_convert_fusion.1
  139.8 0.3 fusion.76
  140.1 0.5 copy-done.3
  140.6 1.1 fusion.44
  141.8 0.6 fusion.67
  142.3 25.0 %all-reduce.2.cloned.1.call-done = bf16[128,2048]{1,0:T(8,128)(2,1)} async-done(((bf16[128,2048]{1,0:T(8,128)(2,1)}), bf16[128,2048]{1,0:T(8,128)(2,1)}) %all-reduce.2.cloned.1.call-update) | async-done | bytes 524304 | tf_op jit(solution)/shard_map/psum | solution.py:220
  167.3 1.9 %copy.167 = bf16[128,2048]{1,0:T(8,128)(2,1)} copy(bf16[128,2048]{1,0:T(8,128)(2,1)} %all-reduce.2.cloned.1.call-done) | data formatting | bytes 1048576
  (83 shorter events, 0.9 us)
Async XLA Ops:
  7.2 132.6 %copy-start = (bf16[256,2048]{1,0:T(8,128)(2,1)S(1)}, bf16[256,2048]{1,0:T(8,128)(2,1)}, u32[]{:S(2)}) copy-start(bf16[256,2048]{1,0:T(8,128)(2,1)} %param.38) | copy-start | bytes 3145732
  7.2 3.1 %copy-start.4 = (bf16[2048,64]{0,1:T(8,128)(2,1)S(1)}, bf16[2048,64]{0,1:T(8,128)(2,1)}, u32[]{:S(2)}) copy-start(bf16[2048,64]{0,1:T(8,128)(2,1)} %param.30) | copy-start | bytes 786436
  7.2 75.4 %all-gather.4.cloned.1.call-start = ((), (), s32[]{:S(2)}) async-start(), calls=%async_computation | async-start | bytes 7864320 | tf_op jit(solution)/shard_map/all_gather | solution.py:158
  7.2 3.1 %copy-start.5 = (bf16[2048,64]{0,1:T(8,128)(2,1)S(1)}, bf16[2048,64]{0,1:T(8,128)(2,1)}, u32[]{:S(2)}) copy-start(bf16[2048,64]{0,1:T(8,128)(2,1)} %param.31) | copy-start | bytes 786436
  7.2 3.2 %copy-start.6 = (bf16[2048,64]{0,1:T(8,128)(2,1)S(1)}, bf16[2048,64]{0,1:T(8,128)(2,1)}, u32[]{:S(2)}) copy-start(bf16[2048,64]{0,1:T(8,128)(2,1)} %param.32) | copy-start | bytes 786436
  10.3 1.4 copy-start.2
  10.4 1.6 copy-start.8
  10.4 72.2 %copy-start.7 = (f32[2048]{0:T(1024)S(1)}, f32[2048]{0:T(1024)}, u32[]{:S(2)}) copy-start(f32[2048]{0:T(1024)} %param.26) | copy-start | bytes 24580
  10.4 1.1 copy-start.1
  11.6 155.7 %all-reduce.2.cloned.1.call-start = ((), (), s32[]{:S(2)}) async-start(), calls=%async_computation.1 | async-start | bytes 1048576 | tf_op jit(solution)/shard_map/psum | solution.py:220
  87.7 2.3 %copy-start.9 = (f32[128]{0:T(128)S(1)}, f32[128]{0:T(128)}, u32[]{:S(2)}) copy-start(f32[128]{0:T(128)} %param.35) | copy-start | bytes 1540
  88.4 38.2 %collective-permute-start = (bf16[1,2,128,256]{3,2,1,0:T(8,128)(2,1)S(1)}, bf16[1,2,128,256]{3,2,1,0:T(8,128)(2,1)S(1)}, u32[]{:S(2)}, u32[]{:S(2)}) collective-permute-start(bf16[1,2,128,256]{3,2,1,0:T(8,128)(2,1)S(1)} %maximum_bitcast_fusion), channel_id=1, source_target_pairs={{0,8},{8,16},{16,24},{1,9},{9,17},{17,25},{2,10},{10,18},{18,26},{... | collective-permute-start | bytes 393224 | tf_op jit(solution)/shard_map/ppermute | solution.py:18
  125.3 2.6 %copy-start.10 = (f32[128]{0:T(128)S(1)}, f32[128]{0:T(128)}, u32[]{:S(2)}) copy-start(f32[128]{0:T(128)} %param.37) | copy-start | bytes 1540
  126.6 10.8 %collective-permute-start.1 = (bf16[2,2,128,256]{3,2,1,0:T(8,128)(2,1)S(1)}, bf16[2,2,128,256]{3,2,1,0:T(8,128)(2,1)S(1)}, u32[]{:S(2)}, u32[]{:S(2)}) collective-permute-start(bf16[2,2,128,256]{3,2,1,0:T(8,128)(2,1)S(1)} %pad_maximum_fusion), channel_id=1, source_target_pairs={{0,16},{8,24},{1,17},{9,25},{2,18},{10,26},{3,19},{11,27},{4,20},{... | collective-permute-start | bytes 786440 | tf_op jit(solution)/shard_map/ppermute | solution.py:18
  137.6 1.9 %copy-start.11 = (f32[2]{0:T(128)S(1)}, f32[2]{0:T(128)}, u32[]{:S(2)}) copy-start(f32[2]{0:T(128)} %param.33) | copy-start | bytes 28
  137.6 2.0 %copy-start.12 = (f32[128]{0:T(128)S(1)}, f32[128]{0:T(128)}, u32[]{:S(2)}) copy-start(f32[128]{0:T(128)} %param.36) | copy-start | bytes 1540
  139.4 1.2 copy-start.3
Sparse Core Ops, SparseCore 0:
  11.7 70.8 all-gather.3
  141.9 25.3 all-reduce.1
where the time goes:
time: 177 us; the launch traced here: 176 us
  waiting for transfers between devices  104 us (59%)
  matrix products  24.6 us (14%)
  blocking collectives  18.9 us (11%)
  between operations  14.6 us (8%)
  local copies, waits for them, and re-layouts  8.18 us (5%)
  starting transfers between devices  2.66 us (2%)
  other arithmetic  2.42 us (1%)
    all_gather x1, waiting for transfers between devices, on_device(): lax.all_gather(stacked, 'fs', axis=2, tiled=True)  70.7 us
    psum x1, waiting for transfers between devices, on_device(): mixed_out = lax.psum(partial_value.astype(jnp.bfloat16), 'tp')  25 us
    all_gather x2, blocking collectives, entering(): pieces = jax.tree.map(lambda part: lax.all_gather(part, axis), value)  18.9 us
    dot_general x2, matrix products, advance(): jnp.einsum('htk,htsk,hsk->hts', query_block, decay, key_block, precision=...  13.9 us
    ppermute x2, waiting for transfers between devices, from_behind(): lax.ppermute(value, axis, [(source, source + steps) for source in range(i...  8.48 us
    unnamed x32, local copies, waits for them, and re-layouts  6.64 us
    dot_general x1, matrix products, on_device(): jnp.einsum('rd,dnc->rnc', normed, lax.all_gather(stacked, 'fs', axis=2, t...  5 us
  transfers between devices with their start and end apart: 4, of which 3 were waited for; matrix products, arithmetic and copies ran while one was open for 11% of the time, Pallas kernels for 0%

commit v1 on v0

v1 whole, which is shorter than its diff:
```python
import functools

import jax
import jax.numpy as jnp
from jax import lax
from jax.experimental import pallas as pl
from jax.experimental.pallas import tpu as pltpu
from jax.sharding import PartitionSpec as P

DK = 64
DV = 128
SUB = 16
EPS = 1e-06
NEG = -1e30
MESH = pl.DeviceIdType.MESH


def dot_nt(a, b):
    return lax.dot_general(a, b, (((1,), (1,)), ((), ())), preferred_element_type=jnp.float32)


def dot_nn(a, b):
    return jnp.dot(a, b, preferred_element_type=jnp.float32)


def partner(f, d, n, sign):
    if n & (n - 1):
        return lax.rem(f + sign * d + n, n)
    out, bit = 0, 1
    while bit < n:
        mine = lax.rem(f // bit, 2)
        out = out + bit * ((1 - mine) if d & bit else mine)
        bit *= 2
    return out


def kernel(
    n_sp, n_fs, n_tp, st_dtype,
    tok, gain, w0, w1, w2, w3, w4, w5, lam, lower, scale, att_gain, rec_gain, aow, row_w,
    mixed, lse,
    wv, aov, rov, wcat, tok_all, nrm, psend, osend, kvall, pr, oprecv, part,
    smat, olocal, qdec, send_st, s_in, s_out, m_s, l_s, acc,
    w_sem, o_sem, tok_s, tok_r, rel_s, rel_r, a_s, a_r, b_s, b_r, kv_s, kv_r, st_s, st_r, op_s, op_r,
):
    z, f, t = lax.axis_index("sp"), lax.axis_index("fs"), lax.axis_index("tp")
    rows, width = tok.shape
    half = rows // n_tp
    heads = n_fs // 2
    nxt, prv = lax.rem(z + 1, n_sp), lax.rem(z + n_sp - 1, n_sp)

    wcopies = [
        pltpu.make_async_copy(w, wv.at[i], w_sem.at[i])
        for i, w in enumerate((w0, w1, w2, w3, w4, w5))
    ]
    for c in wcopies:
        c.start()
    ocopies = [
        pltpu.make_async_copy(aow, aov, o_sem.at[0]),
        pltpu.make_async_copy(row_w, rov, o_sem.at[1]),
    ]

    barrier = pltpu.get_barrier_semaphore()
    for d in range(1, n_fs):
        pl.semaphore_signal(barrier, inc=1, device_id={"fs": partner(f, d, n_fs, 1)}, device_id_type=MESH)
    for d in range(1, n_tp):
        pl.semaphore_signal(barrier, inc=1, device_id={"tp": lax.rem(t + d, n_tp)}, device_id_type=MESH)
    pl.semaphore_signal(barrier, inc=1, device_id={"sp": nxt}, device_id_type=MESH)
    pl.semaphore_signal(barrier, inc=1, device_id={"sp": prv}, device_id_type=MESH)
    pl.semaphore_wait(barrier, n_fs - 1 + n_tp - 1 + 2)

    my_half = pl.ds(pl.multiple_of(t * half, half), half)
    tok_copies = []
    for d in range(1, n_fs):
        c = pltpu.make_async_remote_copy(
            tok.at[my_half], tok_all.at[d - 1, my_half], tok_s.at[d - 1], tok_r.at[d - 1],
            device_id={"fs": partner(f, d, n_fs, 1)}, device_id_type=MESH,
        )
        c.start()
        tok_copies.append(c)
    for c in ocopies:
        c.start()

    for c in wcopies:
        c.wait()
    step = 256
    order = (1, 2, 0, 3, 4, 5)

    @pl.loop(0, width // step)
    def _(i):
        sl = pl.ds(pl.multiple_of(i * step, step), step)
        for j in range(3):
            wcat[sl, j * 2 * DK:(j + 1) * 2 * DK] = jnp.concatenate(
                [wv[order[2 * j], sl, :], wv[order[2 * j + 1], sl, :]], axis=1
            )

    blk = 32

    def project(src_ref):
        @pl.loop(0, rows // blk)
        def _(i):
            sl = pl.ds(pl.multiple_of(i * blk, blk), blk)
            x = src_ref[sl, :].astype(jnp.float32)
            ms = jnp.mean(x * x, axis=-1, keepdims=True)
            nrm[sl, :] = (x * lax.rsqrt(ms + EPS) * gain[...]).astype(jnp.bfloat16)

        return dot_nn(nrm[...], wcat[...]).astype(jnp.bfloat16)

    own = project(tok)
    kvall[z, f] = own[:, : 2 * DK]
    pr[f, 0] = own[:, 2 * DK: 4 * DK]
    pr[f, 1] = own[:, 4 * DK:]

    relays = {}
    for d in range(1, n_fs):
        tok_copies[d - 1].wait_recv()
        for e in range(1, n_tp):
            c = pltpu.make_async_remote_copy(
                tok_all.at[d - 1, my_half], tok_all.at[d - 1, my_half],
                rel_s.at[d - 1, e - 1], rel_r.at[d - 1, e - 1],
                device_id={"tp": lax.rem(t + e, n_tp)}, device_id_type=MESH,
            )
            c.start()
            relays[d, e] = c
        for e in range(1, n_tp):
            relays[d, e].wait_recv()
        got = project(tok_all.at[d - 1])
        to = partner(f, d, n_fs, -1)
        psend[d - 1] = got[:, : 2 * DK]
        osend[d - 1, 0] = got[:, 2 * DK: 4 * DK]
        osend[d - 1, 1] = got[:, 4 * DK:]
        ca = pltpu.make_async_remote_copy(
            psend.at[d - 1], kvall.at[z, f], a_s.at[d - 1], a_r.at[d - 1],
            device_id={"fs": to}, device_id_type=MESH,
        )
        ca.start()
        cb = pltpu.make_async_remote_copy(
            osend.at[d - 1], pr.at[f], b_s.at[d - 1], b_r.at[d - 1],
            device_id={"fs": to}, device_id_type=MESH,
        )
        cb.start()
        relays[d, "a"] = ca
        relays[d, "b"] = cb

    def forward(c, p):
        return pltpu.make_async_remote_copy(
            kvall.at[c, p], kvall.at[c, p], kv_s.at[c, p], kv_r.at[c, p],
            device_id={"sp": nxt}, device_id_type=MESH,
        )

    has_next = z + 1 < n_sp
    for d in range(n_fs):
        if d:
            relays[d, "a"].wait_recv()
        p = partner(f, d, n_fs, 1)

        @pl.when(has_next)
        def _():
            forward(z, p).start()

    for d in range(1, n_fs):
        relays[d, "b"].wait_recv()

    ri_row = lax.broadcasted_iota(jnp.int32, (rows, DV), 0)
    sub_pos = lax.rem(ri_row, SUB)
    tri = (
        lax.broadcasted_iota(jnp.int32, (rows, rows), 0)
        >= lax.broadcasted_iota(jnp.int32, (rows, rows), 1)
    )
    trif = tri.astype(jnp.float32)
    sc = scale[...]
    tails = []
    gates = []
    for h in range(heads):
        rf = jnp.concatenate([pr[2 * h, 1, :, :DK], pr[2 * h + 1, 1, :, :DK]], axis=1).astype(jnp.float32)
        ri = jnp.concatenate([pr[2 * h, 1, :, DK:], pr[2 * h + 1, 1, :, DK:]], axis=1).astype(jnp.float32)
        lb = lower[h: h + 1, :]
        g = sc * jnp.log(lb + (1.0 - lb) * jax.nn.sigmoid(rf))
        kk = 1.0 - jnp.exp(g)
        a = jnp.dot(trif, g, preferred_element_type=jnp.float32, precision=lax.Precision.HIGHEST)
        last = a[rows - 1: rows, :]
        kd = (kk * jnp.exp(last - a)).astype(jnp.bfloat16)
        s_out[h] = dot_nn(ri.T.astype(jnp.bfloat16), kd)
        tails.append(jnp.exp(last))
        gates.append((a, kk, ri))

    def send_state():
        return pltpu.make_async_remote_copy(
            send_st, s_in, st_s, st_r, device_id={"sp": nxt}, device_id_type=MESH
        )

    @pl.when((z == 0) & has_next)
    def _():
        send_st[...] = s_out[...].astype(st_dtype)
        send_state().start()

    def attend(c, first):
        for h in range(heads):
            vh = jnp.concatenate([kvall[c, 2 * h, :, DK:], kvall[c, 2 * h + 1, :, DK:]], axis=1)
            for m in range(2):
                i = 2 * h + m
                sco = dot_nt(pr[i, 0, :, :DK], kvall[c, i, :, :DK]) * DK ** (-0.5)
                if first:
                    sco = jnp.where(tri, sco, NEG)
                    top = jnp.max(sco, axis=-1, keepdims=True)
                    e = jnp.exp(sco - top)
                    l_s[i] = jnp.sum(e, axis=-1, keepdims=True)
                    acc[i] = dot_nn(e.astype(jnp.bfloat16), vh)
                    m_s[i] = top
                else:
                    old = m_s[i]
                    top = jnp.maximum(old, jnp.max(sco, axis=-1, keepdims=True))
                    e = jnp.exp(sco - top)
                    shrink = jnp.exp(old - top)
                    l_s[i] = l_s[i] * shrink + jnp.sum(e, axis=-1, keepdims=True)
                    acc[i] = acc[i] * shrink + dot_nn(e.astype(jnp.bfloat16), vh)
                    m_s[i] = top

    attend(z, True)

    for h in range(heads):
        a, kk, ri = gates[h]
        rq = jnp.concatenate([pr[2 * h, 0, :, DK:], pr[2 * h + 1, 0, :, DK:]], axis=1).astype(jnp.float32)
        qdec[h] = (rq * jnp.exp(a)).astype(jnp.bfloat16)
        smat[h, 0:SUB, :] = jnp.zeros((SUB, rows), jnp.bfloat16)
        for i in range(1, rows // SUB):
            lo = i * SUB
            ref = a[lo - 1: lo, :]
            qd = (rq[lo: lo + SUB] * jnp.exp(a[lo: lo + SUB] - ref)).astype(jnp.bfloat16)
            kd = (kk * jnp.exp(jnp.where(ri_row < lo, ref - a, NEG))).astype(jnp.bfloat16)
            smat[h, lo: lo + SUB, :] = dot_nt(qd, kd).astype(jnp.bfloat16)
        o = dot_nn(smat[h], ri.astype(jnp.bfloat16))
        o = o + jnp.sum(rq * kk, axis=-1, keepdims=True) * ri
        for d in range(1, SUB):
            valid = sub_pos >= d
            dec = jnp.exp(jnp.where(valid, a - pltpu.roll(a, d, 0), NEG))
            col = jnp.sum(rq * dec * pltpu.roll(kk, d, 0), axis=-1, keepdims=True)
            o = o + col * pltpu.roll(ri, d, 0)
        olocal[h] = o

    @pl.loop(0, z)
    def _(s):
        c = z - 1 - s
        for p in range(n_fs):
            cp = forward(c, p)
            cp.wait_recv()

            @pl.when(has_next)
            def _():
                cp.start()

        attend(c, False)

    @pl.when(z > 0)
    def _():
        send_state().wait_recv()

    @pl.when((z > 0) & has_next)
    def _():
        for h in range(heads):
            send_st[h] = (tails[h] * s_in[h].astype(jnp.float32) + s_out[h]).astype(st_dtype)
        send_state().start()

    @pl.when(z > 0)
    def _():
        for h in range(heads):
            olocal[h] = olocal[h] + dot_nt(qdec[h], s_in[h].astype(jnp.bfloat16))

    atts, recs = [], []
    ag, rg = att_gain[...], rec_gain[...]
    lane = lax.broadcasted_iota(jnp.int32, (rows, DV), 1)
    lses = jnp.zeros((rows, DV), jnp.float32)
    for h in range(heads):
        x = acc[2 * h] / l_s[2 * h] - lam[0, h] * (acc[2 * h + 1] / l_s[2 * h + 1])
        ms = jnp.mean(x * x, axis=-1, keepdims=True)
        atts.append((x * lax.rsqrt(ms + EPS) * ag * 0.8).astype(jnp.bfloat16))
        o = olocal[h]
        ms = jnp.mean(o * o, axis=-1, keepdims=True)
        recs.append((o * lax.rsqrt(ms + EPS) * rg).astype(jnp.bfloat16))
        lses = jnp.where(lane == h, m_s[2 * h] + jnp.log(l_s[2 * h]), lses)
    lse[...] = lses.T[:heads, :]
    att = jnp.concatenate(atts, axis=1)
    rec = jnp.concatenate(recs, axis=1)
    for c in ocopies:
        c.wait()
    pieces = part.shape[0]
    cols = part.shape[2]
    swaps = []
    for j in range(pieces):
        sl = slice(j * cols, (j + 1) * cols)
        part[j] = (dot_nn(att, aov[:, sl]) + dot_nn(rec, rov[:, sl])).astype(jnp.bfloat16)
        for e in range(1, n_tp):
            c = pltpu.make_async_remote_copy(
                part.at[j], oprecv.at[e - 1, j], op_s.at[e - 1, j], op_r.at[e - 1, j],
                device_id={"tp": lax.rem(t + e, n_tp)}, device_id_type=MESH,
            )
            c.start()
            swaps.append((j, e, c))
    for j in range(pieces):
        total = part[j].astype(jnp.float32)
        for jj, e, c in swaps:
            if jj == j:
                c.wait_recv()
                total = total + oprecv[e - 1, j].astype(jnp.float32)
        mixed[:, j * cols:(j + 1) * cols] = total.astype(jnp.bfloat16)

    for c in tok_copies:
        c.wait_send()
    for d in range(1, n_fs):
        for e in range(1, n_tp):
            relays[d, e].wait_send()
        relays[d, "a"].wait_send()
        relays[d, "b"].wait_send()
    for _, _, c in swaps:
        c.wait_send()

    @pl.when(has_next)
    def _():
        send_state().wait_send()

        @pl.loop(0, z + 1)
        def _(c):
            for p in range(n_fs):
                forward(c, p).wait_send()


def solution(mesh):
    n_sp, n_fs, n_tp = (mesh.shape[k] for k in ("sp", "fs", "tp"))
    st_dtype = jnp.bfloat16 if n_sp <= 8 else jnp.float32

    def on_device(
        tokens, in_gain, wq, wk, wvv, wrq, wrf, wri, lam, lower, scale, att_gain, rec_gain, aow, row_w
    ):
        rows, width = tokens.shape
        heads = lower.shape[0]
        assert heads * 2 == n_fs and rows % (8 * n_tp) == 0
        vm = pl.BlockSpec(memory_space=pltpu.VMEM)
        sm = pl.BlockSpec(memory_space=pltpu.SMEM)
        hbm = pl.BlockSpec(memory_space=pl.ANY)
        bf, f32 = jnp.bfloat16, jnp.float32
        dma = pltpu.SemaphoreType.DMA
        peers = n_fs - 1
        pieces = 4
        return pl.pallas_call(
            functools.partial(kernel, n_sp, n_fs, n_tp, st_dtype),
            out_shape=(
                jax.ShapeDtypeStruct((rows, width), bf),
                jax.ShapeDtypeStruct((heads, rows), f32),
            ),
            in_specs=[vm, vm] + [hbm] * 6 + [sm, vm, vm, vm, vm, hbm, hbm],
            out_specs=(vm, vm),
            scratch_shapes=[
                pltpu.VMEM((6, width, wq.shape[1]), bf),
                pltpu.VMEM(aow.shape, bf),
                pltpu.VMEM(row_w.shape, bf),
                pltpu.VMEM((width, 6 * DK), bf),
                pltpu.VMEM((peers, rows, width), bf),
                pltpu.VMEM((rows, width), bf),
                pltpu.VMEM((peers, rows, 2 * DK), bf),
                pltpu.VMEM((peers, 2, rows, 2 * DK), bf),
                pltpu.VMEM((n_sp, n_fs, rows, 2 * DK), bf),
                pltpu.VMEM((n_fs, 2, rows, 2 * DK), bf),
                pltpu.VMEM((n_tp - 1, pieces, rows, width // pieces), bf),
                pltpu.VMEM((pieces, rows, width // pieces), bf),
                pltpu.VMEM((heads, rows, rows), bf),
                pltpu.VMEM((heads, rows, DV), f32),
                pltpu.VMEM((heads, rows, DV), bf),
                pltpu.VMEM((heads, DV, DV), st_dtype),
                pltpu.VMEM((heads, DV, DV), st_dtype),
                pltpu.VMEM((heads, DV, DV), f32),
                pltpu.VMEM((2 * heads, rows, 1), f32),
                pltpu.VMEM((2 * heads, rows, 1), f32),
                pltpu.VMEM((2 * heads, rows, DV), f32),
                dma((6,)), dma((2,)),
                dma((peers,)), dma((peers,)),
                dma((peers, n_tp - 1)), dma((peers, n_tp - 1)),
                dma((peers,)), dma((peers,)), dma((peers,)), dma((peers,)),
                dma((n_sp, n_fs)), dma((n_sp, n_fs)),
                dma, dma,
                dma((n_tp - 1, pieces)), dma((n_tp - 1, pieces)),
            ],
            compiler_params=pltpu.CompilerParams(
                collective_id=0, has_side_effects=True, vmem_limit_bytes=60 * 1024 * 1024
            ),
            name="mixer",
        )(
            tokens, in_gain[None], wq, wk, wvv, wrq, wrf, wri, lam[None], lower, scale[:, None],
            att_gain[None], rec_gain[None], aow, row_w,
        )

    col = P(None, ("tp", "fs"))
    return jax.shard_map(
        on_device,
        mesh=mesh,
        in_specs=(
            P(("fs", "sp"), None), P(), col, col, col, col, col, col,
            P("tp"), P("tp", None), P(("fs", "sp")), P(), P(), P("tp", None), P("tp", None),
        ),
        out_specs=(P(("fs", "sp"), None), P("tp", ("fs", "sp"))),
        check_vma=False,
    )
```

time: 177 us -> 50.3 us (0.28)
  waiting for transfers between devices: 104 us -> 0 us
  Pallas kernels: 0 us -> 38.6 us
  matrix products: 24.6 us -> 0 us
  blocking collectives: 18.9 us -> 0 us
  between operations: 14.6 us -> 0.66 us
  local copies, waits for them, and re-layouts: 8.18 us -> 10.9 us
  starting transfers between devices: 2.66 us -> 0 us
  other arithmetic: 2.42 us -> 0 us
    all_gather x1 -> x0, waiting for transfers between devices: 70.7 us -> none  [on_device(): lax.all_gather(stacked, 'fs', axis=2, tiled=True)]
    pallas_call x0 -> x1, Pallas kernels: none -> 38.6 us  [on_device(): pl.pallas_call(functools.partial(kernel, n_sp, n_fs, n_tp, st_dtype), out...]
    psum x1 -> x0, waiting for transfers between devices: 25 us -> none  [on_device(): mixed_out = lax.psum(partial_value.astype(jnp.bfloat16), 'tp')]
    dot_general x20 -> x0, matrix products: 24.6 us -> none  [the longest x2 13.9 us: advance(): jnp.einsum('htk,htsk,hsk->hts', query_block, decay, key_block, precision=...]
    all_gather x2 -> x0, blocking collectives: 18.9 us -> none  [entering(): pieces = jax.tree.map(lambda part: lax.all_gather(part, axis), value)]
    ppermute x2 -> x0, waiting for transfers between devices: 8.48 us -> none  [from_behind(): lax.ppermute(value, axis, [(source, source + steps) for source in range(i...]
    unnamed x32 -> x22, local copies, waits for them, and re-layouts: 6.64 us -> 10.1 us
    ppermute x2 -> x0, starting transfers between devices: 2.58 us -> none  [from_behind(): lax.ppermute(value, axis, [(source, source + steps) for source in range(i...]
  transfers between devices with their start and end apart: 4 -> 0, of which waited for: 3 -> 0; matrix products, arithmetic and copies ran while one was open for 11% -> 0% of each run, Pallas kernels for 0% -> 0%
where the time goes in v1:
time: 50.3 us; the launch traced here: 50.1 us
  Pallas kernels  38.6 us (77%)
  local copies, waits for them, and re-layouts  10.9 us (22%)
  between operations  0.66 us (1%)
    pallas_call x1, Pallas kernels, on_device(): pl.pallas_call(functools.partial(kernel, n_sp, n_fs, n_tp, st_dtype), out...  38.6 us
    unnamed x22, local copies, waits for them, and re-layouts  10.1 us

profile of v1, /device:TPU:25, one launch (start us, length us, event | category | flops | bytes accessed | tf_op | source)
XLA Modules:
  0.0 50.1 jit_solution(1345517088892235549)
XLA Ops:
  0.6 0.0 copy-start.6
  0.6 0.6 %copy-done.6 = f32[128]{0:T(128)S(1)} copy-done((f32[128]{0:T(128)S(1)}, f32[128]{0:T(128)}, u32[]{:S(2)}) %copy-start.6) | copy-done | bytes 536
  1.3 0.7 %copy.23.scale = f32[128,1]{1,0:T(8,128)} copy(f32[128,1]{0,1:T(1,128)S(1)} %bitcast.6) | data formatting | bytes 1024 | tf_op jit(solution)/shard_map/broadcast_in_dim | solution.py:386
  2.0 0.0 copy-start
  2.0 2.0 %copy.17.w0 = bf16[2048,64]{1,0:T(8,128)(2,1)} copy(bf16[2048,64]{0,1:T(8,128)(2,1)} %param.17) | data formatting | bytes 524288 | tf_op args[2]
  4.0 0.0 copy-done
  4.0 0.0 copy-start.1
  4.0 1.0 %copy.18.w1 = bf16[2048,64]{1,0:T(8,128)(2,1)} copy(bf16[2048,64]{0,1:T(8,128)(2,1)S(1)} %copy-done) | data formatting | bytes 524288 | tf_op args[3]
  5.0 0.0 copy-done.1
  5.0 0.0 copy-start.2
  5.0 1.0 %copy.19.w2 = bf16[2048,64]{1,0:T(8,128)(2,1)} copy(bf16[2048,64]{0,1:T(8,128)(2,1)S(1)} %copy-done.1) | data formatting | bytes 524288 | tf_op args[4]
  6.0 0.0 copy-done.2
  6.0 0.0 copy-start.3
  6.0 1.0 %copy.20.w3 = bf16[2048,64]{1,0:T(8,128)(2,1)} copy(bf16[2048,64]{0,1:T(8,128)(2,1)S(1)} %copy-done.2) | data formatting | bytes 524288 | tf_op args[5]
  7.1 0.0 copy-done.3
  7.1 0.0 copy-start.4
  7.1 1.0 %copy.21.w4 = bf16[2048,64]{1,0:T(8,128)(2,1)} copy(bf16[2048,64]{0,1:T(8,128)(2,1)S(1)} %copy-done.3) | data formatting | bytes 524288 | tf_op args[6]
  8.1 0.0 copy-done.4
  8.1 1.0 %copy.22.w5 = bf16[2048,64]{1,0:T(8,128)(2,1)} copy(bf16[2048,64]{0,1:T(8,128)(2,1)S(1)} %copy-done.4) | data formatting | bytes 524288 | tf_op args[7]
  9.1 38.6 %mixer.1 = (bf16[128,2048]{1,0:T(8,128)(2,1)}, f32[2,128]{1,0:T(2,128)}) custom-call(bf16[128,2048]{1,0:T(8,128)(2,1)} %tok.1, f32[1,2048]{1,0:T(1,128)} %bitcast.5, bf16[2048,64]{1,0:T(8,128)(2,1)} %copy.17.w0, bf16[2048,64]{1,0:T(8,128)(2,1)} %copy.18.w1, bf16[2048,64]{1,0:T(8,128)(2,1)} %copy.19.w2, bf16[2048,64]{1,0:T(8,128)(2,1)} %copy.20.w3, ...), custom_call_target="tpu_custom_call" | custom-call | tf_op jit(solution)/shard_map/mixer/pallas_call | solution.py:343
  47.7 0.0 copy-start.5
  47.7 1.9 %copy.26 = bf16[128,2048]{1,0:T(8,128)(2,1)} copy(bf16[128,2048]{1,0:T(8,128)(2,1)} %get-tuple-element.4) | data formatting | bytes 1048576
  49.6 0.0 copy-done.5
  49.6 0.6 %copy.27 = f32[2,128]{1,0:T(2,128)} copy(f32[2,128]{1,0:T(2,128)S(1)} %copy-done.5) | data formatting | bytes 2048
Async XLA Ops:
  0.6 0.7 %copy-start.6 = (f32[128]{0:T(128)S(1)}, f32[128]{0:T(128)}, u32[]{:S(2)}) copy-start(f32[128]{0:T(128)} %param.25) | copy-start | bytes 1540
  2.0 2.0 %copy-start = (bf16[2048,64]{0,1:T(8,128)(2,1)S(1)}, bf16[2048,64]{0,1:T(8,128)(2,1)}, u32[]{:S(2)}) copy-start(bf16[2048,64]{0,1:T(8,128)(2,1)} %param.18) | copy-start | bytes 786436
  4.0 1.0 %copy-start.1 = (bf16[2048,64]{0,1:T(8,128)(2,1)S(1)}, bf16[2048,64]{0,1:T(8,128)(2,1)}, u32[]{:S(2)}) copy-start(bf16[2048,64]{0,1:T(8,128)(2,1)} %param.19) | copy-start | bytes 786436
  5.0 1.0 %copy-start.2 = (bf16[2048,64]{0,1:T(8,128)(2,1)S(1)}, bf16[2048,64]{0,1:T(8,128)(2,1)}, u32[]{:S(2)}) copy-start(bf16[2048,64]{0,1:T(8,128)(2,1)} %param.20) | copy-start | bytes 786436
  6.0 1.0 %copy-start.3 = (bf16[2048,64]{0,1:T(8,128)(2,1)S(1)}, bf16[2048,64]{0,1:T(8,128)(2,1)}, u32[]{:S(2)}) copy-start(bf16[2048,64]{0,1:T(8,128)(2,1)} %param.21) | copy-start | bytes 786436
  7.1 1.0 %copy-start.4 = (bf16[2048,64]{0,1:T(8,128)(2,1)S(1)}, bf16[2048,64]{0,1:T(8,128)(2,1)}, u32[]{:S(2)}) copy-start(bf16[2048,64]{0,1:T(8,128)(2,1)} %param.22) | copy-start | bytes 786436
  47.7 1.9 %copy-start.5 = (f32[2,128]{1,0:T(2,128)S(1)}, f32[2,128]{1,0:T(2,128)}, u32[]{:S(2)}) copy-start(f32[2,128]{1,0:T(2,128)} %get-tuple-element.5) | copy-start | bytes 3076

commit v2 on v1

v2 whole, which is shorter than its diff:
```python
import functools

import jax
import jax.numpy as jnp
from jax import lax
from jax.experimental import pallas as pl
from jax.experimental.pallas import tpu as pltpu
from jax.sharding import PartitionSpec as P

DK = 64
DV = 128
SUB = 16
GROUPS = 2
EPS = 1e-06
NEG = -1e30
MESH = pl.DeviceIdType.MESH


def dot_nt(a, b):
    return lax.dot_general(a, b, (((1,), (1,)), ((), ())), preferred_element_type=jnp.float32)


def dot_nn(a, b):
    return jnp.dot(a, b, preferred_element_type=jnp.float32)


def partner(f, d, n, sign):
    if n & (n - 1):
        return lax.rem(f + sign * d + n, n)
    out, bit = 0, 1
    while bit < n:
        mine = lax.rem(f // bit, 2)
        out = out + bit * ((1 - mine) if d & bit else mine)
        bit *= 2
    return out


def kernel(
    n_sp, n_fs, n_tp, st_dtype,
    tok, gain, w0, w1, w2, w3, w4, w5, lam, lower, scale, att_gain, rec_gain, aow, row_w,
    parts, lse,
    aov, rov, wcat, tok_all, nrm, psend, osend, kvall, pr,
    smat, olocal, qdec, gate, send_st, s_in, s_out, m_s, l_s, acc,
    w_sem, o_sem, tok_s, tok_r, rel_s, rel_r, a_s, a_r, b_s, b_r, kv_s, kv_r, st_s, st_r, op_s, op_r,
):
    z, f, t = lax.axis_index("sp"), lax.axis_index("fs"), lax.axis_index("tp")
    rows, width = tok.shape
    heads = n_fs // 2
    grp = rows // GROUPS
    mine = grp // n_tp
    sub = mine // 2
    nxt, prv = lax.rem(z + 1, n_sp), lax.rem(z + n_sp - 1, n_sp)
    has_next = z + 1 < n_sp
    hop = n_fs == 4

    order = (2, 0, 1, 3, 4, 5)
    wcopies = [
        pltpu.make_async_copy(w, wcat.at[pl.ds(order[i] * DK, DK)], w_sem.at[i])
        for i, w in enumerate((w0, w1, w2, w3, w4, w5))
    ]
    for c in wcopies:
        c.start()
    ocopies = [
        pltpu.make_async_copy(aow, aov, o_sem.at[0]),
        pltpu.make_async_copy(row_w, rov, o_sem.at[1]),
    ]

    barrier = pltpu.get_barrier_semaphore()
    for d in range(1, n_fs):
        pl.semaphore_signal(barrier, inc=1, device_id={"fs": partner(f, d, n_fs, 1)}, device_id_type=MESH)
    for d in range(1, n_tp):
        pl.semaphore_signal(barrier, inc=1, device_id={"tp": lax.rem(t + d, n_tp)}, device_id_type=MESH)
    pl.semaphore_signal(barrier, inc=1, device_id={"sp": nxt}, device_id_type=MESH)
    pl.semaphore_signal(barrier, inc=1, device_id={"sp": prv}, device_id_type=MESH)
    pl.semaphore_wait(barrier, n_fs - 1 + n_tp - 1 + 2)

    def span(g, u):
        return pl.ds(pl.multiple_of(g * grp + t * mine + u * sub, sub), sub)

    def token_copy(g, d, u):
        if hop and d == 3:
            src, to = (tok_all.at[0], 2) if u == 0 else (tok_all.at[1], 1)
        else:
            src, to = tok, d
        return pltpu.make_async_remote_copy(
            src.at[span(g, u)], tok_all.at[d - 1, span(g, u)],
            tok_s.at[g, d - 1, u], tok_r.at[g, d - 1, u],
            device_id={"fs": partner(f, to, n_fs, 1)}, device_id_type=MESH,
        )

    def relay(g, d, u, e):
        return pltpu.make_async_remote_copy(
            tok_all.at[d - 1, span(g, u)], tok_all.at[d - 1, span(g, u)],
            rel_s.at[g, d - 1, u, e - 1], rel_r.at[g, d - 1, u, e - 1],
            device_id={"tp": lax.rem(t + e, n_tp)}, device_id_type=MESH,
        )

    def relay_wait(g, d, u, e):
        other = lax.rem(t + n_tp - e, n_tp)
        at = pl.ds(pl.multiple_of(g * grp + other * mine + u * sub, sub), sub)
        pltpu.make_async_remote_copy(
            tok_all.at[d - 1, at], tok_all.at[d - 1, at],
            rel_s.at[g, d - 1, u, e - 1], rel_r.at[g, d - 1, u, e - 1],
            device_id={"tp": lax.rem(t + e, n_tp)}, device_id_type=MESH,
        ).wait_recv()

    def direct(g):
        if hop:
            seq = [(1, 0), (2, 1), (1, 1), (2, 0)]
        else:
            seq = [(d, u) for d in range(1, n_fs) for u in range(2)]
        for d, u in seq:
            token_copy(g, d, u).start()

    def arrive(g, d, u):
        token_copy(g, d, u).wait_recv()
        if hop and (d, u) in ((1, 0), (2, 1)):
            token_copy(g, 3, u).start()
        for e in range(1, n_tp):
            relay(g, d, u, e).start()

    def first_arrivals(g):
        if hop:
            arrive(g, 1, 0)
            arrive(g, 2, 1)

    def last_arrivals(g):
        if hop:
            seq = [(1, 1), (2, 0), (3, 0), (3, 1)]
        else:
            seq = [(d, u) for d in range(1, n_fs) for u in range(2)]
        for d, u in seq:
            arrive(g, d, u)
        for d in range(1, n_fs):
            for u in range(2):
                for e in range(1, n_tp):
                    relay_wait(g, d, u, e)

    blk = min(32, grp)

    def normalise(src_ref, first, to):
        @pl.loop(0, grp // blk)
        def _(i):
            x = src_ref[pl.ds(pl.multiple_of(first + i * blk, blk), blk), :].astype(jnp.float32)
            ms = jnp.mean(x * x, axis=-1, keepdims=True)
            nrm[pl.ds(pl.multiple_of(to + i * blk, blk), blk), :] = (
                x * lax.rsqrt(ms + EPS) * gain[...]
            ).astype(jnp.bfloat16)

    def back(g, d):
        to = partner(f, d, n_fs, -1)
        return (
            pltpu.make_async_remote_copy(
                psend.at[g, d - 1], kvall.at[z, g, f], a_s.at[g, d - 1], a_r.at[g, d - 1],
                device_id={"fs": to}, device_id_type=MESH,
            ),
            pltpu.make_async_remote_copy(
                osend.at[g, d - 1], pr.at[f, g], b_s.at[g, d - 1], b_r.at[g, d - 1],
                device_id={"fs": to}, device_id_type=MESH,
            ),
        )

    def project(g):
        for d in range(1, n_fs):
            normalise(tok_all.at[d - 1], g * grp, d * grp)
        got = dot_nt(nrm[...], wcat[...]).astype(jnp.bfloat16)
        for d in range(1, n_fs):
            lo = d * grp
            psend[g, d - 1] = got[lo: lo + grp, : 2 * DK]
            osend[g, d - 1, 0] = got[lo: lo + grp, 2 * DK: 4 * DK]
            osend[g, d - 1, 1] = got[lo: lo + grp, 4 * DK:]
        kvall[z, g, f] = got[:grp, : 2 * DK]
        pr[f, g, 0] = got[:grp, 2 * DK: 4 * DK]
        pr[f, g, 1] = got[:grp, 4 * DK:]
        for d in range(1, n_fs):
            back(g, d)[0].start()
        for d in range(1, n_fs):
            back(g, d)[1].start()

    def chain(c, g):
        return pltpu.make_async_remote_copy(
            kvall.at[c, g], kvall.at[c, g], kv_s.at[c, g], kv_r.at[c, g],
            device_id={"sp": nxt}, device_id_type=MESH,
        )

    def own_chain(g):
        for d in range(1, n_fs):
            back(g, d)[0].wait_recv()

        @pl.when(has_next)
        def _():
            chain(z, g).start()

    def pass_on(c, g):
        chain(c, g).wait_recv()

        @pl.when(has_next)
        def _():
            chain(c, g).start()

    def forward(k):
        s, g = k // GROUPS, k % GROUPS
        if s < n_sp - 1:
            @pl.when(z > s)
            def _():
                pass_on(z - 1 - s, g)

    direct(0)
    for c in ocopies:
        c.start()
    normalise(tok, 0, 0)
    first_arrivals(0)
    for g in range(1, GROUPS):
        direct(g)
    for c in wcopies:
        c.wait()
    last_arrivals(0)
    project(0)
    for g in range(1, GROUPS):
        normalise(tok, g * grp, 0)
        first_arrivals(g)
        own_chain(g - 1)
        last_arrivals(g)
        project(g)
    forward(0)
    own_chain(GROUPS - 1)
    for g in range(GROUPS):
        for d in range(1, n_fs):
            back(g, d)[1].wait_recv()

    def column(i, j, part):
        return pr[i, :, j, :, part * DK:(part + 1) * DK].reshape(rows, DK)

    def wide(h, j, part):
        return jnp.concatenate([column(2 * h, j, part), column(2 * h + 1, j, part)], axis=1)

    row_at = lax.broadcasted_iota(jnp.int32, (rows, DV), 0)
    sub_pos = lax.rem(row_at, SUB)
    tri = (
        lax.broadcasted_iota(jnp.int32, (rows, rows), 0)
        >= lax.broadcasted_iota(jnp.int32, (rows, rows), 1)
    )
    trif = tri.astype(jnp.float32)
    sc = jnp.broadcast_to(scale[...], (DV, rows)).T
    tails = []
    for h in range(heads):
        rf = wide(h, 1, 0).astype(jnp.float32)
        ri = wide(h, 1, 1).astype(jnp.float32)
        lb = lower[h: h + 1, :]
        g = sc * jnp.log(lb + (1.0 - lb) * jax.nn.sigmoid(rf))
        kk = 1.0 - jnp.exp(g)
        a = jnp.dot(trif, g, preferred_element_type=jnp.float32, precision=lax.Precision.HIGHEST)
        last = a[rows - 1: rows, :]
        kd = (kk * jnp.exp(last - a)).astype(jnp.bfloat16)
        s_out[h] = dot_nn(ri.T.astype(jnp.bfloat16), kd)
        tails.append(jnp.exp(last))
        gate[h, 0] = a
        gate[h, 1] = kk

    def send_state():
        return pltpu.make_async_remote_copy(
            send_st, s_in, st_s, st_r, device_id={"sp": nxt}, device_id_type=MESH
        )

    @pl.when((z == 0) & has_next)
    def _():
        send_st[...] = s_out[...].astype(st_dtype)
        send_state().start()

    def carry(when):
        @pl.when(when)
        def _():
            send_state().wait_recv()

        @pl.when(when & has_next)
        def _():
            for h in range(heads):
                send_st[h] = (tails[h] * s_in[h].astype(jnp.float32) + s_out[h]).astype(st_dtype)
            send_state().start()

    def attend(c, first):
        for h in range(heads):
            vh = jnp.concatenate(
                [
                    kvall[c, :, 2 * h, :, DK:].reshape(rows, DK),
                    kvall[c, :, 2 * h + 1, :, DK:].reshape(rows, DK),
                ],
                axis=1,
            )
            for m in range(2):
                i = 2 * h + m
                keys = kvall[c, :, i, :, :DK].reshape(rows, DK)
                sco = dot_nt(column(i, 0, 0), keys) * DK ** (-0.5)
                if first:
                    sco = jnp.where(tri, sco, NEG)
                    top = jnp.max(sco, axis=-1, keepdims=True)
                    e = jnp.exp(sco - top)
                    l_s[i] = jnp.sum(e, axis=-1, keepdims=True)
                    acc[i] = dot_nn(e.astype(jnp.bfloat16), vh)
                    m_s[i] = top
                else:
                    old = m_s[i]
                    top = jnp.maximum(old, jnp.max(sco, axis=-1, keepdims=True))
                    e = jnp.exp(sco - top)
                    shrink = jnp.exp(old - top)
                    l_s[i] = l_s[i] * shrink + jnp.sum(e, axis=-1, keepdims=True)
                    acc[i] = acc[i] * shrink + dot_nn(e.astype(jnp.bfloat16), vh)
                    m_s[i] = top

    def recur(h):
        a, kk = gate[h, 0], gate[h, 1]
        ri = wide(h, 1, 1).astype(jnp.float32)
        rq = wide(h, 0, 1).astype(jnp.float32)
        qdec[h] = (rq * jnp.exp(a)).astype(jnp.bfloat16)
        smat[h, 0:SUB, :] = jnp.zeros((SUB, rows), jnp.bfloat16)
        for i in range(1, rows // SUB):
            lo = i * SUB
            ref = a[lo - 1: lo, :]
            qd = (rq[lo: lo + SUB] * jnp.exp(a[lo: lo + SUB] - ref)).astype(jnp.bfloat16)
            kd = (kk * jnp.exp(jnp.where(row_at < lo, ref - a, NEG))).astype(jnp.bfloat16)
            smat[h, lo: lo + SUB, :] = dot_nt(qd, kd).astype(jnp.bfloat16)
        o = dot_nn(smat[h], ri.astype(jnp.bfloat16))
        o = o + jnp.sum(rq * kk, axis=-1, keepdims=True) * ri
        for d in range(1, SUB):
            dec = jnp.exp(jnp.where(sub_pos >= d, a - pltpu.roll(a, d, 0), NEG))
            col = jnp.sum(rq * dec * pltpu.roll(kk, d, 0), axis=-1, keepdims=True)
            o = o + col * pltpu.roll(ri, d, 0)
        olocal[h] = o

    forward(1)
    carry(z == 1)
    forward(2)
    attend(z, True)
    forward(3)
    recur(0)
    carry(z == 2)
    forward(4)

    @pl.when(z > 0)
    def _():
        attend(z - 1, False)

    forward(5)
    for h in range(1, heads):
        recur(h)

    @pl.loop(1, z)
    def _(s):
        c = z - 1 - s

        @pl.when(s >= 3)
        def _():
            for g in range(GROUPS):
                pass_on(c, g)

        attend(c, False)

    carry(z > 2)

    @pl.when(z > 0)
    def _():
        for h in range(heads):
            olocal[h] = olocal[h] + dot_nt(qdec[h], s_in[h].astype(jnp.bfloat16))

    atts, recs = [], []
    ag, rg = att_gain[...], rec_gain[...]
    lane = lax.broadcasted_iota(jnp.int32, (rows, DV), 1)
    lses = jnp.zeros((rows, DV), jnp.float32)
    for h in range(heads):
        x = acc[2 * h] / l_s[2 * h] - lam[0, h] * (acc[2 * h + 1] / l_s[2 * h + 1])
        ms = jnp.mean(x * x, axis=-1, keepdims=True)
        atts.append((x * lax.rsqrt(ms + EPS) * ag * 0.8).astype(jnp.bfloat16))
        o = olocal[h]
        ms = jnp.mean(o * o, axis=-1, keepdims=True)
        recs.append((o * lax.rsqrt(ms + EPS) * rg).astype(jnp.bfloat16))
        lses = jnp.where(lane == h, m_s[2 * h] + jnp.log(l_s[2 * h]), lses)
    lse[...] = lses.T[:heads, :]
    att = jnp.concatenate(atts, axis=1)
    rec = jnp.concatenate(recs, axis=1)
    for c in ocopies:
        c.wait()
    pieces = 4
    cols = width // pieces
    swaps = []
    for j in range(pieces):
        sl = slice(j * cols, (j + 1) * cols)
        parts[0, :, sl] = (dot_nn(att, aov[:, sl]) + dot_nn(rec, rov[:, sl])).astype(jnp.bfloat16)
        for e in range(1, n_tp):
            c = pltpu.make_async_remote_copy(
                parts.at[0, :, sl], parts.at[e, :, sl], op_s.at[e - 1, j], op_r.at[e - 1, j],
                device_id={"tp": lax.rem(t + e, n_tp)}, device_id_type=MESH,
            )
            c.start()
            swaps.append(c)

    for g in range(GROUPS):
        for d in range(1, n_fs):
            for u in range(2):
                token_copy(g, d, u).wait_send()
                for e in range(1, n_tp):
                    relay(g, d, u, e).wait_send()
            for c in back(g, d):
                c.wait_send()

    @pl.when(has_next)
    def _():
        send_state().wait_send()

        @pl.loop(0, z + 1)
        def _(c):
            for g in range(GROUPS):
                chain(c, g).wait_send()

    for c in swaps:
        c.wait()


def finish(parts, lse_in, mixed, lse):
    total = parts[0].astype(jnp.float32)
    for e in range(1, parts.shape[0]):
        total = total + parts[e].astype(jnp.float32)
    mixed[...] = total.astype(jnp.bfloat16)
    lse[...] = lse_in[...]


def solution(mesh):
    n_sp, n_fs, n_tp = (mesh.shape[k] for k in ("sp", "fs", "tp"))
    st_dtype = jnp.bfloat16 if n_sp <= 8 else jnp.float32

    def on_device(
        tokens, in_gain, wq, wk, wvv, wrq, wrf, wri, lam, lower, scale, att_gain, rec_gain, aow, row_w
    ):
        rows, width = tokens.shape
        heads = lower.shape[0]
        assert heads * 2 == n_fs and rows % (8 * n_tp) == 0
        vm = pl.BlockSpec(memory_space=pltpu.VMEM)
        sm = pl.BlockSpec(memory_space=pltpu.SMEM)
        hbm = pl.BlockSpec(memory_space=pl.ANY)
        bf, f32 = jnp.bfloat16, jnp.float32
        dma = pltpu.SemaphoreType.DMA
        peers = n_fs - 1
        pieces = 4
        grp = rows // GROUPS
        parts, lse = pl.pallas_call(
            functools.partial(kernel, n_sp, n_fs, n_tp, st_dtype),
            out_shape=(
                jax.ShapeDtypeStruct((n_tp, rows, width), bf),
                jax.ShapeDtypeStruct((heads, rows), f32),
            ),
            in_specs=[vm, vm] + [hbm] * 6 + [sm, vm, vm, vm, vm, hbm, hbm],
            out_specs=(vm, vm),
            scratch_shapes=[
                pltpu.VMEM(aow.shape, bf),
                pltpu.VMEM(row_w.shape, bf),
                pltpu.VMEM((6 * DK, width), bf),
                pltpu.VMEM((peers, rows, width), bf),
                pltpu.VMEM((n_fs * grp, width), bf),
                pltpu.VMEM((GROUPS, peers, grp, 2 * DK), bf),
                pltpu.VMEM((GROUPS, peers, 2, grp, 2 * DK), bf),
                pltpu.VMEM((n_sp, GROUPS, n_fs, grp, 2 * DK), bf),
                pltpu.VMEM((n_fs, GROUPS, 2, grp, 2 * DK), bf),
                pltpu.VMEM((heads, rows, rows), bf),
                pltpu.VMEM((heads, rows, DV), f32),
                pltpu.VMEM((heads, rows, DV), bf),
                pltpu.VMEM((heads, 2, rows, DV), f32),
                pltpu.VMEM((heads, DV, DV), st_dtype),
                pltpu.VMEM((heads, DV, DV), st_dtype),
                pltpu.VMEM((heads, DV, DV), f32),
                pltpu.VMEM((2 * heads, rows, 1), f32),
                pltpu.VMEM((2 * heads, rows, 1), f32),
                pltpu.VMEM((2 * heads, rows, DV), f32),
                dma((6,)), dma((2,)),
                dma((GROUPS, peers, 2)), dma((GROUPS, peers, 2)),
                dma((GROUPS, peers, 2, n_tp - 1)), dma((GROUPS, peers, 2, n_tp - 1)),
                dma((GROUPS, peers)), dma((GROUPS, peers)), dma((GROUPS, peers)), dma((GROUPS, peers)),
                dma((n_sp, GROUPS)), dma((n_sp, GROUPS)),
                dma, dma,
                dma((n_tp - 1, pieces)), dma((n_tp - 1, pieces)),
            ],
            compiler_params=pltpu.CompilerParams(
                collective_id=0, has_side_effects=True, vmem_limit_bytes=56 * 1024 * 1024
            ),
            name="mixer",
        )(
            tokens, in_gain[None], wq.T, wk.T, wvv.T, wrq.T, wrf.T, wri.T, lam[None], lower, scale[None],
            att_gain[None], rec_gain[None], aow, row_w,
        )
        half = width // 2
        return pl.pallas_call(
            finish,
            grid=(2,),
            out_shape=(
                jax.ShapeDtypeStruct((rows, width), bf),
                jax.ShapeDtypeStruct((heads, rows), f32),
            ),
            in_specs=[
                pl.BlockSpec((n_tp, rows, half), lambda i: (0, 0, i)),
                pl.BlockSpec((heads, rows), lambda i: (0, 0)),
            ],
            out_specs=(
                pl.BlockSpec((rows, half), lambda i: (0, i)),
                pl.BlockSpec((heads, rows), lambda i: (0, 0)),
            ),
            name="finish",
        )(parts, lse)

    col = P(None, ("tp", "fs"))
    return jax.shard_map(
        on_device,
        mesh=mesh,
        in_specs=(
            P(("fs", "sp"), None), P(), col, col, col, col, col, col,
            P("tp"), P("tp", None), P(("fs", "sp")), P(), P(), P("tp", None), P("tp", None),
        ),
        out_specs=(P(("fs", "sp"), None), P("tp", ("fs", "sp"))),
        check_vma=False,
    )
```

time: 50.3 us -> 46 us (0.915)
  local copies, waits for them, and re-layouts: 10.9 us -> 0 us
  Pallas kernels: 38.6 us -> 45.2 us
    unnamed x22 -> x0, local copies, waits for them, and re-layouts: 10.1 us -> none
    pallas_call x1, Pallas kernels: 38.6 us -> 43.2 us  [on_device(): pl.pallas_call(functools.partial(kernel, n_sp, n_fs, n_tp, st_dtype), out...]
    pallas_call x0 -> x1, Pallas kernels: none -> 1.99 us  [on_device(): pl.pallas_call(finish, grid=(2,), out_shape=(jax.ShapeDtypeStruct((rows,...]
    broadcast_in_dim x1 -> x0, local copies, waits for them, and re-layouts: 0.73 us -> none  [on_device(): scale[:, None]]
where the time goes in v2:
time: 46 us; the launch traced here: 45.9 us
  Pallas kernels  45.2 us (98%)
  between operations  0.64 us (1%)
    pallas_call x1, Pallas kernels, on_device(): pl.pallas_call(functools.partial(kernel, n_sp, n_fs, n_tp, st_dtype), out...  43.2 us
    pallas_call x1, Pallas kernels, on_device(): pl.pallas_call(finish, grid=(2,), out_shape=(jax.ShapeDtypeStruct((rows,...  1.99 us

profile of v2, /device:TPU:25, one launch (start us, length us, event | category | flops | bytes accessed | tf_op | source)
XLA Modules:
  0.0 45.9 jit_solution(13917413637980824605)
XLA Ops:
  0.6 43.2 %mixer.1 = (bf16[2,128,2048]{2,1,0:T(8,128)(2,1)}, f32[2,128]{1,0:T(2,128)}) custom-call(bf16[128,2048]{1,0:T(8,128)(2,1)} %tok.1, f32[1,2048]{1,0:T(1,128)} %bitcast.17, bf16[64,2048]{1,0:T(8,128)(2,1)} %bitcast.11, bf16[64,2048]{1,0:T(8,128)(2,1)} %bitcast.12, bf16[64,2048]{1,0:T(8,128)(2,1)} %bitcast.13, bf16[64,2048]{1,0:T(8,128)(2,1)} %bitcast.14, ...), custom_call_target="tpu_custom_call" | custom-call | tf_op jit(solution)/shard_map/mixer/pallas_call | solution.py:444
  43.9 2.0 %finish.1 = (bf16[128,2048]{1,0:T(8,128)(2,1)}, f32[2,128]{1,0:T(2,128)}) custom-call(bf16[2,128,2048]{2,1,0:T(8,128)(2,1)} %get-tuple-element.4.parts, f32[2,128]{1,0:T(2,128)} %get-tuple-element.5.lse_in), custom_call_target="tpu_custom_call" | custom-call | tf_op jit(solution)/shard_map/finish/pallas_call | solution.py:489

commit v3 on v1

--- a/solution.py
+++ b/solution.py
@@ -37,8 +37,8 @@
 def kernel(
     n_sp, n_fs, n_tp, st_dtype,
     tok, gain, w0, w1, w2, w3, w4, w5, lam, lower, scale, att_gain, rec_gain, aow, row_w,
-    mixed, lse,
-    wv, aov, rov, wcat, tok_all, nrm, psend, osend, kvall, pr, oprecv, part,
+    parts, lse,
+    aov, rov, wcat, tok_all, nrm, psend, osend, kvall, pr,
     smat, olocal, qdec, send_st, s_in, s_out, m_s, l_s, acc,
     w_sem, o_sem, tok_s, tok_r, rel_s, rel_r, a_s, a_r, b_s, b_r, kv_s, kv_r, st_s, st_r, op_s, op_r,
 ):
@@ -48,8 +48,9 @@
     heads = n_fs // 2
     nxt, prv = lax.rem(z + 1, n_sp), lax.rem(z + n_sp - 1, n_sp)
 
+    order = (2, 0, 1, 3, 4, 5)
     wcopies = [
-        pltpu.make_async_copy(w, wv.at[i], w_sem.at[i])
+        pltpu.make_async_copy(w, wcat.at[pl.ds(order[i] * DK, DK)], w_sem.at[i])
         for i, w in enumerate((w0, w1, w2, w3, w4, w5))
     ]
     for c in wcopies:
@@ -82,16 +83,6 @@
 
     for c in wcopies:
         c.wait()
-    step = 256
-    order = (1, 2, 0, 3, 4, 5)
-
-    @pl.loop(0, width // step)
-    def _(i):
-        sl = pl.ds(pl.multiple_of(i * step, step), step)
-        for j in range(3):
-            wcat[sl, j * 2 * DK:(j + 1) * 2 * DK] = jnp.concatenate(
-                [wv[order[2 * j], sl, :], wv[order[2 * j + 1], sl, :]], axis=1
-            )
 
     blk = 32
 
@@ -103,7 +94,7 @@
             ms = jnp.mean(x * x, axis=-1, keepdims=True)
             nrm[sl, :] = (x * lax.rsqrt(ms + EPS) * gain[...]).astype(jnp.bfloat16)
 
-        return dot_nn(nrm[...], wcat[...]).astype(jnp.bfloat16)
+        return dot_nt(nrm[...], wcat[...]).astype(jnp.bfloat16)
 
     own = project(tok)
     kvall[z, f] = own[:, : 2 * DK]
@@ -167,7 +158,7 @@
         >= lax.broadcasted_iota(jnp.int32, (rows, rows), 1)
     )
     trif = tri.astype(jnp.float32)
-    sc = scale[...]
+    sc = jnp.broadcast_to(scale[...], (DV, rows)).T
     tails = []
     gates = []
     for h in range(heads):
@@ -282,26 +273,19 @@
     rec = jnp.concatenate(recs, axis=1)
     for c in ocopies:
         c.wait()
-    pieces = part.shape[0]
-    cols = part.shape[2]
+    pieces = 4
+    cols = width // pieces
     swaps = []
     for j in range(pieces):
         sl = slice(j * cols, (j + 1) * cols)
-        part[j] = (dot_nn(att, aov[:, sl]) + dot_nn(rec, rov[:, sl])).astype(jnp.bfloat16)
+        parts[0, :, sl] = (dot_nn(att, aov[:, sl]) + dot_nn(rec, rov[:, sl])).astype(jnp.bfloat16)
         for e in range(1, n_tp):
             c = pltpu.make_async_remote_copy(
-                part.at[j], oprecv.at[e - 1, j], op_s.at[e - 1, j], op_r.at[e - 1, j],
+                parts.at[0, :, sl], parts.at[e, :, sl], op_s.at[e - 1, j], op_r.at[e - 1, j],
                 device_id={"tp": lax.rem(t + e, n_tp)}, device_id_type=MESH,
             )
             c.start()
-            swaps.append((j, e, c))
-    for j in range(pieces):
-        total = part[j].astype(jnp.float32)
-        for jj, e, c in swaps:
-            if jj == j:
-                c.wait_recv()
-                total = total + oprecv[e - 1, j].astype(jnp.float32)
-        mixed[:, j * cols:(j + 1) * cols] = total.astype(jnp.bfloat16)
+            swaps.append(c)
 
     for c in tok_copies:
         c.wait_send()
@@ -310,9 +294,6 @@
             relays[d, e].wait_send()
         relays[d, "a"].wait_send()
         relays[d, "b"].wait_send()
-    for _, _, c in swaps:
-        c.wait_send()
-
     @pl.when(has_next)
     def _():
         send_state().wait_send()
@@ -321,6 +302,17 @@
         def _(c):
             for p in range(n_fs):
                 forward(c, p).wait_send()
+
+    for c in swaps:
+        c.wait()
+
+
+def finish(parts, lse_in, mixed, lse):
+    total = parts[0].astype(jnp.float32)
+    for e in range(1, parts.shape[0]):
+        total = total + parts[e].astype(jnp.float32)
+    mixed[...] = total.astype(jnp.bfloat16)
+    lse[...] = lse_in[...]
 
 
 def solution(mesh):
@@ -340,27 +332,24 @@
         dma = pltpu.SemaphoreType.DMA
         peers = n_fs - 1
         pieces = 4
-        return pl.pallas_call(
+        parts, lse = pl.pallas_call(
             functools.partial(kernel, n_sp, n_fs, n_tp, st_dtype),
             out_shape=(
-                jax.ShapeDtypeStruct((rows, width), bf),
+                jax.ShapeDtypeStruct((n_tp, rows, width), bf),
                 jax.ShapeDtypeStruct((heads, rows), f32),
             ),
             in_specs=[vm, vm] + [hbm] * 6 + [sm, vm, vm, vm, vm, hbm, hbm],
             out_specs=(vm, vm),
             scratch_shapes=[
-                pltpu.VMEM((6, width, wq.shape[1]), bf),
                 pltpu.VMEM(aow.shape, bf),
                 pltpu.VMEM(row_w.shape, bf),
-                pltpu.VMEM((width, 6 * DK), bf),
+                pltpu.VMEM((6 * DK, width), bf),
                 pltpu.VMEM((peers, rows, width), bf),
                 pltpu.VMEM((rows, width), bf),
                 pltpu.VMEM((peers, rows, 2 * DK), bf),
                 pltpu.VMEM((peers, 2, rows, 2 * DK), bf),
                 pltpu.VMEM((n_sp, n_fs, rows, 2 * DK), bf),
                 pltpu.VMEM((n_fs, 2, rows, 2 * DK), bf),
-                pltpu.VMEM((n_tp - 1, pieces, rows, width // pieces), bf),
-                pltpu.VMEM((pieces, rows, width // pieces), bf),
                 pltpu.VMEM((heads, rows, rows), bf),
                 pltpu.VMEM((heads, rows, DV), f32),
                 pltpu.VMEM((heads, rows, DV), bf),
@@ -379,13 +368,31 @@
                 dma((n_tp - 1, pieces)), dma((n_tp - 1, pieces)),
             ],
             compiler_params=pltpu.CompilerParams(
-                collective_id=0, has_side_effects=True, vmem_limit_bytes=60 * 1024 * 1024
+                collective_id=0, has_side_effects=True, vmem_limit_bytes=56 * 1024 * 1024
             ),
             name="mixer",
         )(
-            tokens, in_gain[None], wq, wk, wvv, wrq, wrf, wri, lam[None], lower, scale[:, None],
+            tokens, in_gain[None], wq.T, wk.T, wvv.T, wrq.T, wrf.T, wri.T, lam[None], lower, scale[None],
             att_gain[None], rec_gain[None], aow, row_w,
         )
+        half = width // 2
+        return pl.pallas_call(
+            finish,
+            grid=(2,),
+            out_shape=(
+                jax.ShapeDtypeStruct((rows, width), bf),
+                jax.ShapeDtypeStruct((heads, rows), f32),
+            ),
+            in_specs=[
+                pl.BlockSpec((n_tp, rows, half), lambda i: (0, 0, i)),
+                pl.BlockSpec((heads, rows), lambda i: (0, 0)),
+            ],
+            out_specs=(
+                pl.BlockSpec((rows, half), lambda i: (0, i)),
+                pl.BlockSpec((heads, rows), lambda i: (0, 0)),
+            ),
+            name="finish",
+        )(parts, lse)
 
     col = P(None, ("tp", "fs"))
     return jax.shard_map(

time: 50.3 us -> 41.5 us (0.83)
  local copies, waits for them, and re-layouts: 10.9 us -> 0 us
  Pallas kernels: 38.6 us -> 40.7 us
    unnamed x22 -> x0, local copies, waits for them, and re-layouts: 10.1 us -> none
    pallas_call x0 -> x1, Pallas kernels: none -> 1.99 us  [on_device(): pl.pallas_call(finish, grid=(2,), out_shape=(jax.ShapeDtypeStruct((rows,...]
    broadcast_in_dim x1 -> x0, local copies, waits for them, and re-layouts: 0.73 us -> none  [on_device(): scale[:, None]]
where the time goes in v3:
time: 41.5 us; the launch traced here: 41.4 us
  Pallas kernels  40.7 us (98%)
  between operations  0.64 us (2%)
    pallas_call x1, Pallas kernels, on_device(): pl.pallas_call(functools.partial(kernel, n_sp, n_fs, n_tp, st_dtype), out...  38.7 us
    pallas_call x1, Pallas kernels, on_device(): pl.pallas_call(finish, grid=(2,), out_shape=(jax.ShapeDtypeStruct((rows,...  1.99 us

profile of v3, /device:TPU:25, one launch (start us, length us, event | category | flops | bytes accessed | tf_op | source)
XLA Modules:
  0.0 41.4 jit_solution(11981322441260880517)
XLA Ops:
  0.6 38.7 %mixer.1 = (bf16[2,128,2048]{2,1,0:T(8,128)(2,1)}, f32[2,128]{1,0:T(2,128)}) custom-call(bf16[128,2048]{1,0:T(8,128)(2,1)} %tok.1, f32[1,2048]{1,0:T(1,128)} %bitcast.17, bf16[64,2048]{1,0:T(8,128)(2,1)} %bitcast.11, bf16[64,2048]{1,0:T(8,128)(2,1)} %bitcast.12, bf16[64,2048]{1,0:T(8,128)(2,1)} %bitcast.13, bf16[64,2048]{1,0:T(8,128)(2,1)} %bitcast.14, ...), custom_call_target="tpu_custom_call" | custom-call | tf_op jit(solution)/shard_map/mixer/pallas_call | solution.py:335
  39.4 2.0 %finish.1 = (bf16[128,2048]{1,0:T(8,128)(2,1)}, f32[2,128]{1,0:T(2,128)}) custom-call(bf16[2,128,2048]{2,1,0:T(8,128)(2,1)} %get-tuple-element.4.parts, f32[2,128]{1,0:T(2,128)} %get-tuple-element.5.lse_in), custom_call_target="tpu_custom_call" | custom-call | tf_op jit(solution)/shard_map/finish/pallas_call | solution.py:379
